TPU v7x, 32 devices: a whole 2x2x4 slice. The times are simulated.
32 devices in a mesh: sp: 4 (over y, x), tp: 8 (over z, core).
Axes of the slice: x: 2, y: 2, z: 4, core: 2. Of those that a mesh axis runs over, the one named last changes fastest.
Arguments:
- resid: bfloat16 [2048, 2048], P(('sp', 'tp')), may hold values from -6 to 6
- query_a: bfloat16 [2048, 16, 128], P('sp', 'tp'), may hold values from -16 to 16
- key_a: bfloat16 [2048, 16, 128], P('sp', 'tp'), may hold values from -16 to 16
- value_a: bfloat16 [2048, 16, 128], P('sp', 'tp'), may hold values from -6 to 6
- query_b: bfloat16 [2048, 16, 64], P('sp', 'tp'), may hold values from -16 to 16
- key_b: bfloat16 [2048, 16, 64], P('sp', 'tp'), may hold values from -16 to 16
- value_b: bfloat16 [2048, 16, 64], P('sp', 'tp'), may hold values from -6 to 6
- mix_a: float32 [16], P('tp'), may hold values from 0.3 to 0.8
- mix_b: float32 [16], P('tp'), may hold values from 0.3 to 0.8
- head_gain_a: float32 [128], replicated, may hold values from 0.1 to 1.9
- head_gain_b: float32 [64], replicated, may hold values from 0.1 to 1.9
- proj_a: bfloat16 [2048, 2048], P('tp'), may hold values from -0.109375 to 0.109375
- proj_b: bfloat16 [1024, 2048], P('tp'), may hold values from -0.109375 to 0.109375
- norm_gain: float32 [2048], replicated, may hold values from 0.1 to 1.9
- route_ids: int32 [2048, 2], P(('sp', 'tp')), may hold values from 0 to 3, all different within a row; in each aligned block of 64 rows (0 to 63, 64 to 127, ...) at most 48 rows name the same one
- route_weights: float32 [2048, 2], P(('sp', 'tp')), may hold values from 0.2 to 1
- expert_gate: bfloat16 [4, 2048, 6144], P('sp', None, 'tp'), may hold values from -0.125 to 0.125
- expert_up: bfloat16 [4, 2048, 6144], P('sp', None, 'tp'), may hold values from -0.125 to 0.125
- expert_down: bfloat16 [4, 6144, 2048], P('sp', 'tp'), may hold values from -0.078125 to 0.078125
Outputs:
- out: bfloat16 [2048, 2048], P(('sp', 'tp'))
Inputs may be any that keep to these rules, and one draw needn't show every extreme that they name: `route_ids`: each row names 2 different experts. Within the rows of one device (aligned blocks of 64 rows) no expert is named by more than 48 rows, and in every draw some device's block names some expert exactly 48 times.
All inputs are finite; a program needn't handle non-finite values.
Results may differ from a plain program's by a relative error of at most 0.02.
Values may be sent and summed in bfloat16 or wider, within the bound.
No kernel may reach another device: no remote copies, remote signals or barrier semaphores. Data moves between devices by JAX's collectives and lax.ppermute only.
A program may use at most 128 MiB of HBM per device.

v0:
```python
import math

import jax
import jax.numpy as jnp
from jax import lax
from jax.sharding import PartitionSpec as P

EPS = 1e-06
NEG = -1e30
HEAD_SCALE = 1.0 - (0.8 - 0.6 * math.exp(-0.3))
KEY_STEP = 512


def partner(value, axis, apart):
    return lax.ppermute(value, axis, [(i, i ^ 1 << apart) for i in range(lax.axis_size(axis))])


def rms_scaled(values, gain):
    return values * lax.rsqrt(jnp.mean(values * values, axis=-1, keepdims=True) + EPS) * gain


def slot_numbers(route_rows, experts, capacity):
    count, top_count = route_rows.shape
    flat = route_rows.reshape(count * top_count)
    onehot = (flat[:, None] == jnp.arange(experts, dtype=jnp.int32)[None, :]).astype(jnp.int32)
    ranks = jnp.sum((jnp.cumsum(onehot, axis=0) - onehot) * onehot, axis=1)
    return (flat * capacity + ranks).reshape(count, top_count)


def empty_map(count, heads, width):
    return (
        jnp.zeros((count, heads, width), jnp.float32),
        jnp.full((heads, count), NEG, jnp.float32),
        jnp.zeros((heads, count), jnp.float32),
    )


def empty_group(query, value):
    return (
        empty_map(query.shape[0], query.shape[1], value.shape[2]),
        empty_map(query.shape[0], query.shape[1], value.shape[2]),
    )


def map_update(state, query, keys, values, allowed, scale):
    weighted, maximum, sums = state
    scores = jnp.einsum("qhd,khd->hqk", query, keys, preferred_element_type=jnp.float32) * scale
    scores = jnp.where(allowed[None], scores, NEG)
    fresh = jnp.maximum(maximum, jnp.max(scores, axis=2))
    weights = jnp.where(allowed[None], jnp.exp(scores - fresh[:, :, None]), 0.0)
    factor = jnp.exp(maximum - fresh)
    sums = sums * factor + jnp.sum(weights, axis=2)
    added = jnp.einsum(
        "hqk,khv->qhv", weights.astype(jnp.bfloat16), values, preferred_element_type=jnp.float32
    )
    weighted = weighted * jnp.transpose(factor)[:, :, None] + added
    return (weighted, fresh, sums)


def group_update(states, query, keys, values, allowed):
    width = query.shape[2] // 2
    scale = 1.0 / math.sqrt(width)
    return tuple(
        (
            map_update(
                states[which],
                query[:, :, which * width : (which + 1) * width],
                keys[:, :, which * width : (which + 1) * width],
                values,
                allowed,
                scale,
            )
            for which in range(2)
        )
    )


def set_update(carry, queries, pieces):
    rows_a, rows_b, query_pos = queries
    piece_key_a, piece_value_a, piece_key_b, piece_value_b = pieces
    length = piece_key_a.shape[0]
    step = math.gcd(length, KEY_STEP)
    latest = query_pos[-1]

    def inner(index, states):
        first = index * step

        def compute(current):
            keys_a = lax.dynamic_slice_in_dim(piece_key_a, first, step, 0)
            values_a = lax.dynamic_slice_in_dim(piece_value_a, first, step, 0)
            keys_b = lax.dynamic_slice_in_dim(piece_key_b, first, step, 0)
            values_b = lax.dynamic_slice_in_dim(piece_value_b, first, step, 0)
            key_pos = first + jnp.arange(step, dtype=jnp.int32)
            allowed = key_pos[None, :] <= query_pos[:, None]
            return (
                group_update(current[0], rows_a, keys_a, values_a, allowed),
                group_update(current[1], rows_b, keys_b, values_b, allowed),
            )

        return lax.cond(first <= latest, compute, lambda current: current, states)

    return lax.fori_loop(0, length // step, inner, carry)


def finish_group(states, mix, gain):
    outputs = [state[0] / jnp.transpose(state[2])[:, :, None] for state in states]
    mixed = outputs[0] - mix[None, :, None] * outputs[1]
    normed = rms_scaled(mixed, gain) * HEAD_SCALE
    return normed.astype(jnp.bfloat16).reshape(mixed.shape[0], -1)


def per_device(
    resid,
    query_a,
    key_a,
    value_a,
    query_b,
    key_b,
    value_b,
    mix_a,
    mix_b,
    head_gain_a,
    head_gain_b,
    proj_a,
    proj_b,
    norm_gain,
    route_ids,
    route_weights,
    expert_gate,
    expert_up,
    expert_down,
):
    seq_rows = query_a.shape[0]
    sp_ways = lax.axis_size("sp")
    place = lax.axis_index("sp")
    positions = place * seq_rows + jnp.arange(seq_rows, dtype=jnp.int32)
    levels = sp_ways.bit_length() - 1
    half = seq_rows // 2
    moved = jnp.concatenate(
        [query_a[half:].reshape(half, -1), query_b[half:].reshape(half, -1)], axis=1
    )
    for bit in range(levels):
        moved = partner(moved, "sp", bit)
    split_at = query_a.shape[1] * query_a.shape[2]
    far_a = moved[:, :split_at].reshape(half, query_a.shape[1], query_a.shape[2])
    far_b = moved[:, split_at:].reshape(half, query_b.shape[1], query_b.shape[2])
    far_pos = (sp_ways - 1 - place) * seq_rows + half + jnp.arange(half, dtype=jnp.int32)
    query_sets = ((query_a[:half], query_b[:half], positions[:half]), (far_a, far_b, far_pos))

    def fold_keys(carry, pieces):
        return tuple(
            (set_update(states, queries, pieces) for states, queries in zip(carry, query_sets))
        )

    initial = tuple(
        (
            (empty_group(queries[0], value_a), empty_group(queries[1], value_b))
            for queries in query_sets
        )
    )
    results = fold_keys(
        initial,
        (
            lax.all_gather(key_a, "sp", axis=0, tiled=True),
            lax.all_gather(value_a, "sp", axis=0, tiled=True),
            lax.all_gather(key_b, "sp", axis=0, tiled=True),
            lax.all_gather(value_b, "sp", axis=0, tiled=True),
        ),
    )
    finished = [
        (finish_group(states[0], mix_a, head_gain_a), finish_group(states[1], mix_b, head_gain_b))
        for states in results
    ]
    returned = jnp.concatenate([finished[1][0], finished[1][1]], axis=1)
    for bit in range(levels):
        returned = partner(returned, "sp", bit)
    width_a = finished[0][0].shape[1]
    heads_out_a = jnp.concatenate([finished[0][0], returned[:, :width_a]], axis=0)
    heads_out_b = jnp.concatenate([finished[0][1], returned[:, width_a:]], axis=0)
    width = resid.shape[1]
    tok_rows = resid.shape[0]
    top_count = route_ids.shape[1]
    capacity = 3 * top_count * tok_rows // (2 * sp_ways)
    own_slots = slot_numbers(route_ids, sp_ways, capacity)
    term = jnp.dot(heads_out_a, proj_a, preferred_element_type=jnp.float32)
    term = term + jnp.dot(heads_out_b, proj_b, preferred_element_type=jnp.float32)
    mixed = resid.astype(jnp.float32) + lax.psum_scatter(
        lax.optimization_barrier(term.astype(jnp.bfloat16))
        .astype(jnp.float32)
        .astype(jnp.bfloat16),
        "tp",
        scatter_dimension=0,
        tiled=True,
    ).astype(jnp.float32)
    normed = rms_scaled(mixed, norm_gain).astype(jnp.bfloat16)
    lookup = jnp.arange(sp_ways * capacity, dtype=jnp.int32)[:, None]
    spread = jnp.zeros((sp_ways * capacity, tok_rows), jnp.float32)
    for which in range(top_count):
        spread = spread + (own_slots[:, which][None, :] == lookup).astype(jnp.float32)
    outgoing = jnp.dot(
        spread.astype(jnp.bfloat16), normed, preferred_element_type=jnp.float32
    ).astype(jnp.bfloat16)
    arrived = lax.all_to_all(
        outgoing.reshape(sp_ways, capacity, width), "sp", split_axis=0, concat_axis=0, tiled=True
    )
    piece = lax.all_gather(arrived.reshape(sp_ways * capacity, width), "tp", axis=0, tiled=True)
    gate = jnp.dot(piece, expert_gate[0], preferred_element_type=jnp.float32)
    upward = jnp.dot(piece, expert_up[0], preferred_element_type=jnp.float32)
    hidden = (jax.nn.silu(gate) * upward).astype(jnp.bfloat16)
    term = jnp.dot(hidden, expert_down[0], preferred_element_type=jnp.float32)
    summed = lax.psum_scatter(
        lax.optimization_barrier(term.astype(jnp.bfloat16))
        .astype(jnp.float32)
        .astype(jnp.bfloat16),
        "tp",
        scatter_dimension=0,
        tiled=True,
    )
    finished_rows = summed.reshape(sp_ways, capacity, width)
    back = lax.all_to_all(finished_rows, "sp", split_axis=0, concat_axis=0, tiled=True)
    picked = jnp.take(back.reshape(sp_ways * capacity, width), own_slots.reshape(-1), axis=0)
    picked = picked.reshape(tok_rows, top_count, width)
    output = mixed + jnp.sum(route_weights[:, :, None] * picked.astype(jnp.float32), axis=1)
    return output.astype(jnp.bfloat16)


def solution(mesh):
    placed = (
        P(("sp", "tp"), None),
        P("sp", "tp", None),
        P("sp", "tp", None),
        P("sp", "tp", None),
        P("sp", "tp", None),
        P("sp", "tp", None),
        P("sp", "tp", None),
        P("tp"),
        P("tp"),
        P(),
        P(),
        P("tp", None),
        P("tp", None),
        P(),
        P(("sp", "tp"), None),
        P(("sp", "tp"), None),
        P("sp", None, "tp"),
        P("sp", None, "tp"),
        P("sp", "tp", None),
    )
    return jax.shard_map(
        per_device, mesh=mesh, in_specs=placed, out_specs=P(("sp", "tp"), None), check_vma=False
    )
```

profile of v0, /device:TPU:0, one launch (start us, length us, event | category | flops | bytes accessed | tf_op | source)
XLA Modules:
  0.0 423.4 jit_solution(7599969802928675392)
XLA Ops:
  6.5 2.0 copy.58
  8.6 1.8 copy.60
  11.7 1.5 fusion.160
  14.0 3.0 collective-permute-start
  19.5 4.5 %collective-permute-done = bf16[256,384]{0,1:T(8,128)(2,1)} collective-permute-done((bf16[256,384]{0,1:T(8,128)(2,1)}, bf16[256,384]{0,1:T(8,128)(2,1)}, u32[]{:S(2)}, u32[]{:S(2)}) %collective-permute-start) | collective-permute-done | bytes 196640 | tf_op jit(solution)/shard_map/ppermute | solution.py:15
  25.3 16.1 %all_gather.17 = bf16[2048,2,64]{0,2,1:T(8,128)(2,1)} all-gather(bf16[512,2,64]{0,2,1:T(8,128)(2,1)} %param.32), channel_id=1, replica_groups=mesh['sp'=4,'tp'=8] {'sp'}, dimensions={0}, use_global_device_ids=true | all-gather | bytes 655360 | tf_op jit(solution)/shard_map/all_gather | solution.py:166
  41.4 10.7 %all_gather.18 = bf16[2048,2,64]{0,2,1:T(8,128)(2,1)} all-gather(bf16[512,2,64]{0,2,1:T(8,128)(2,1)} %param.33), channel_id=1, replica_groups=mesh['sp'=4,'tp'=8] {'sp'}, dimensions={0}, use_global_device_ids=true | all-gather | bytes 655360 | tf_op jit(solution)/shard_map/all_gather | solution.py:167
  53.4 17.1 %all-gather.6.cloned.1.call-done = bf16[2048,2,128]{0,2,1:T(8,128)(2,1)} async-done(((bf16[512,2,128]{0,2,1:T(8,128)(2,1)}), bf16[2048,2,128]{0,2,1:T(8,128)(2,1)}) %all-gather.6.cloned.1.call-update) | async-done | bytes 1048592 | tf_op jit(solution)/shard_map/all_gather | solution.py:165
  74.9 65.4 %while.72 = (s32[]{:T(128)}, f32[256,2,128]{0,2,1:T(8,128)S(1)}, f32[2,256]{1,0:T(2,128)S(1)}, f32[2,256]{1,0:T(2,128)}, f32[256,2,128]{0,2,1:T(8,128)}, /*index...) while((s32[]{:T(128)}, f32[256,2,128]{0,2,1:T(8,128)S(1)}, ...), condition=%wide.region_24.25_spmd.clone, body=%wide.region_13.24_spmd.clone.sunk | while | flops 311958272 | bytes 29590432 | solution.py:102
  75.5 15.7 %conditional.6 = ((f32[256,2,128]{0,2,1:T(8,128)S(1)}, f32[2,256]{1,0:T(2,128)S(1)}, f32[2,256]{1,0:T(2,128)}, f32[256,2,128]{0,2,1:T(8,128)}, f32[2,256]{1,0:T(...) conditional(s32[]{:T(128)} %convert_element_type.167, ...), branch_computations={%region_14.14_spmd, %region_15.23_spmd} | conditional | flops 311958272 | bytes 29588914 | solution.py:100
  75.7 2.3 fusion.157
  87.0 1.9 fusion.76
  88.9 1.9 fusion.77
  91.8 15.8 %conditional.6 = ((f32[256,2,128]{0,2,1:T(8,128)S(1)}, f32[2,256]{1,0:T(2,128)S(1)}, f32[2,256]{1,0:T(2,128)}, f32[256,2,128]{0,2,1:T(8,128)}, f32[2,256]{1,0:T(...) conditional(s32[]{:T(128)} %convert_element_type.167, ...), branch_computations={%region_14.14_spmd, %region_15.23_spmd} | conditional | flops 311958272 | bytes 29588914 | solution.py:100
  92.0 2.2 fusion.157
  103.3 1.9 fusion.76
  105.3 1.9 fusion.77
  108.2 15.7 %conditional.6 = ((f32[256,2,128]{0,2,1:T(8,128)S(1)}, f32[2,256]{1,0:T(2,128)S(1)}, f32[2,256]{1,0:T(2,128)}, f32[256,2,128]{0,2,1:T(8,128)}, f32[2,256]{1,0:T(...) conditional(s32[]{:T(128)} %convert_element_type.167, ...), branch_computations={%region_14.14_spmd, %region_15.23_spmd} | conditional | flops 311958272 | bytes 29588914 | solution.py:100
  108.4 2.2 fusion.157
  119.7 1.9 fusion.76
  121.6 1.9 fusion.77
  124.5 15.7 %conditional.6 = ((f32[256,2,128]{0,2,1:T(8,128)S(1)}, f32[2,256]{1,0:T(2,128)S(1)}, f32[2,256]{1,0:T(2,128)}, f32[256,2,128]{0,2,1:T(8,128)}, f32[2,256]{1,0:T(...) conditional(s32[]{:T(128)} %convert_element_type.167, ...), branch_computations={%region_14.14_spmd, %region_15.23_spmd} | conditional | flops 311958272 | bytes 29588914 | solution.py:100
  124.7 2.2 fusion.157
  136.0 1.9 fusion.76
  137.9 1.9 fusion.77
  145.4 19.4 %while.71 = (s32[]{:T(128)}, f32[256,2,128]{0,2,1:T(8,128)S(1)}, f32[2,256]{1,0:T(2,128)S(1)}, f32[2,256]{1,0:T(2,128)}, f32[256,2,128]{0,2,1:T(8,128)}, /*index...) while((s32[]{:T(128)}, f32[256,2,128]{0,2,1:T(8,128)S(1)}, ...), condition=%wide.region_11.12_spmd, body=%wide.region_0.11_spmd.sunk | while | flops 311958016 | bytes 29587348 | solution.py:102
  146.0 16.9 %conditional.5 = ((f32[256,2,128]{0,2,1:T(8,128)S(1)}, f32[2,256]{1,0:T(2,128)S(1)}, f32[2,256]{1,0:T(2,128)}, f32[256,2,128]{0,2,1:T(8,128)}, f32[2,256]{1,0:T(...) conditional(s32[]{:T(128)} %convert_element_type.166, ...), branch_computations={%region_1.0_spmd, %region_2.10_spmd} | conditional | flops 311958016 | bytes 29586862 | solution.py:100
  147.4 2.3 fusion.153
  158.6 2.0 fusion.12
  160.6 1.8 fusion.13
  169.0 2.7 collective-permute-start.2
  171.8 4.7 %collective-permute-done.2 = bf16[256,384]{0,1:T(8,128)(2,1)S(1)} collective-permute-done((bf16[256,384]{0,1:T(8,128)(2,1)S(1)}, bf16[256,384]{0,1:T(8,128)(2,1)S(1)}, u32[]{:S(2)}, u32[]{:S(2)}) %collective-permute-start.2) | collective-permute-done | bytes 196640 | tf_op jit(solution)/shard_map/ppermute | solution.py:15
  176.5 3.0 collective-permute-start.3
  179.4 3.9 collective-permute-done.3
  184.1 2.1 add_convert_fusion
  187.2 36.5 %reduce-scatter.3.cloned.1.call-done = bf16[64,2048]{1,0:T(8,128)(2,1)} async-done(((bf16[512,2048]{1,0:T(8,128)(2,1)}), bf16[64,2048]{1,0:T(8,128)(2,1)}) %reduce-scatter.3.cloned.1.call-update) | async-done | bytes 262160 | tf_op jit(solution)/shard_map/reduce_scatter | solution.py:187
  226.3 12.3 %all_to_all.10 = bf16[4,48,2048]{2,1,0:T(8,128)(2,1)} all-to-all(bf16[4,48,2048]{2,1,0:T(8,128)(2,1)S(1)} %bitcast.127), channel_id=1, replica_groups=mesh['sp'=4,'tp'=8] {'sp'}, dimensions={0} | all-to-all | bytes 1572864 | tf_op jit(solution)/shard_map/all_to_all | solution.py:203
  238.8 63.9 %all-gather.8.cloned.1.call-done = bf16[1536,2048]{1,0:T(8,128)(2,1)} async-done(((bf16[192,2048]{1,0:T(8,128)(2,1)}), bf16[1536,2048]{1,0:T(8,128)(2,1)}) %all-gather.8.cloned.1.call-update) | async-done | bytes 6291472 | tf_op jit(solution)/shard_map/all_gather | solution.py:206
  302.7 8.2 %fusion.132 = f32[1536,768]{1,0:T(8,128)S(1)} fusion(bf16[1536,2048]{1,0:T(8,128)(2,1)} %all-gather.8.cloned.1.call-done, bf16[1,2048,768]{2,1,0:T(8,128)(2,1)} %param.43), kind=kOutput, calls=%fused_computation.172 | convolution fusion | flops 4831838208 | bytes 14155776 | tf_op jit(solution)/shard_map/dot_general | solution.py:207
  311.0 5.6 %multiply_convert_fusion = bf16[1536,768]{1,0:T(8,128)(2,1)S(1)} fusion(f32[1536,768]{1,0:T(8,128)S(1)} %fusion.132, bf16[1536,2048]{1,0:T(8,128)(2,1)S(1)} %copy-done.24, bf16[1,2048,768]{2,1,0:T(8,128)(2,1)S(1)} %copy-done.25), kind=kOutput, calls=%fused_computation.168 | convolution fusion | flops 4838916096 | bytes 16515072 | tf_op jit(solution)/shard_map/dot_general | solution.py:208
  316.6 7.1 %convolution_convert_fusion = bf16[1536,2048]{1,0:T(8,128)(2,1)} fusion(bf16[1536,768]{1,0:T(8,128)(2,1)S(1)} %multiply_convert_fusion, bf16[1,768,2048]{2,1,0:T(8,128)(2,1)S(1)} %copy-done), kind=kOutput, calls=%fused_computation.167 | convolution fusion | flops 4834983936 | bytes 11796480 | tf_op jit(solution)/shard_map/dot_general | solution.py:210
  323.7 68.5 %reduce-scatter.5.cloned.1.call-done = bf16[192,2048]{1,0:T(8,128)(2,1)} async-done(((bf16[1536,2048]{1,0:T(8,128)(2,1)}), bf16[192,2048]{1,0:T(8,128)(2,1)}) %reduce-scatter.5.cloned.1.call-update) | async-done | bytes 786448 | tf_op jit(solution)/shard_map/reduce_scatter | solution.py:211
  392.3 4.2 all-to-all-start.1
  396.9 8.8 %all-to-all-done.1 = bf16[4,48,2048]{2,1,0:T(8,128)(2,1)} async-done(((bf16[4,48,2048]{2,1,0:T(8,128)(2,1)}), bf16[4,48,2048]{2,1,0:T(8,128)(2,1)}, u32[]{:S(2)}, u32[]{:S(2)}) %all-to-all-start.1) | async-done | bytes 786464 | tf_op jit(solution)/shard_map/all_to_all | solution.py:220
  405.7 3.5 gather_fusion
  409.2 2.2 gather.7
  411.4 3.7 multiply_reduce_fusion
  415.1 1.8 add_convert_fusion.1
  (278 shorter events, 74.6 us)
Async XLA Ops:
  6.5 310.0 %copy-start = (bf16[1,768,2048]{2,1,0:T(8,128)(2,1)S(1)}, bf16[1,768,2048]{2,1,0:T(8,128)(2,1)}, u32[]{:S(2)}) copy-start(bf16[1,768,2048]{2,1,0:T(8,128)(2,1)} %param.45) | copy-start | bytes 9437188
  6.5 46.9 %all-gather.4.cloned.1.call-start = ((), (), s32[]{:S(2)}) async-start(), calls=%async_computation.4 | async-start | bytes 1310720 | tf_op jit(solution)/shard_map/all_gather | solution.py:164
  8.5 62.0 %all-gather.6.cloned.1.call-start = ((), (), s32[]{:S(2)}) async-start(), calls=%async_computation.5 | async-start | bytes 1310720 | tf_op jit(solution)/shard_map/all_gather | solution.py:165
  10.4 213.3 %reduce-scatter.3.cloned.1.call-start = ((), (), s32[]{:S(2)}) async-start(), calls=%async_computation.6 | async-start | bytes 2359296 | tf_op jit(solution)/shard_map/reduce_scatter | solution.py:187
  14.0 10.0 %collective-permute-start = (bf16[256,384]{0,1:T(8,128)(2,1)}, bf16[256,384]{0,1:T(8,128)(2,1)}, u32[]{:S(2)}, u32[]{:S(2)}) collective-permute-start(bf16[256,384]{0,1:T(8,128)(2,1)} %pad_maximum_fusion), channel_id=1, source_target_pairs={{0,8},{8,0},{16,24},{24,16},{1,9},{9,1},{17,25},{25,17},{2,10},{10... | collective-permute-start | bytes 589832 | tf_op jit(solution)/shard_map/ppermute | solution.py:15
  24.0 28.1 %collective-permute-start.1 = (bf16[256,384]{0,1:T(8,128)(2,1)}, bf16[256,384]{0,1:T(8,128)(2,1)S(1)}, u32[]{:S(2)}, u32[]{:S(2)}) collective-permute-start(bf16[256,384]{0,1:T(8,128)(2,1)} %collective-permute-done), channel_id=1, source_target_pairs={{0,16},{8,24},{16,0},{24,8},{1,17},{9,25},{17,1},{25,9},{2,18},{10... | collective-permute-start | bytes 589832 | tf_op jit(solution)/shard_map/ppermute | solution.py:15
  78.5 4.7 %copy-start.1 = (f32[2,256,512]{1,2,0:T(8,128)S(1)}, f32[2,256,512]{1,2,0:T(8,128)}, u32[]{:S(2)}) copy-start(f32[2,256,512]{1,2,0:T(8,128)} %get-tuple-element.1138) | copy-start | bytes 3145732 | tf_op jit(solution)/shard_map/while/body/eval_jaxpr/cond
  78.5 5.4 %copy-start.18 = (f32[2,256]{1,0:T(2,128)S(1)}, f32[2,256]{1,0:T(2,128)}, u32[]{:S(2)}) copy-start(f32[2,256]{1,0:T(2,128)} %copy-done.17) | copy-start | bytes 6148 | tf_op jit(solution)/shard_map/while/body/eval_jaxpr/cond
  78.5 8.0 %copy-start.3 = (bf16[2048,2,128]{0,2,1:T(8,128)(2,1)S(1)}, bf16[2048,2,128]{0,2,1:T(8,128)(2,1)}, u32[]{:S(2)}) copy-start(bf16[2048,2,128]{0,2,1:T(8,128)(2,1)} %get-tuple-element.863) | copy-start | bytes 3145732 | tf_op jit(solution)/shard_map/while/body/eval_jaxpr/cond
  78.5 8.0 %copy-start.10 = (f32[256,2,128]{0,2,1:T(8,128)S(1)}, f32[256,2,128]{0,2,1:T(8,128)}, u32[]{:S(2)}) copy-start(f32[256,2,128]{0,2,1:T(8,128)} %get-tuple-element.865) | copy-start | bytes 786436 | tf_op jit(solution)/shard_map/while/body/eval_jaxpr/cond
  78.6 8.0 %copy-start.19 = (f32[256,2]{0,1:T(2,128)S(1)}, f32[256,2]{0,1:T(2,128)}, u32[]{:S(2)}) copy-start(f32[256,2]{0,1:T(2,128)} %get-tuple-element.1107) | copy-start | bytes 6148 | tf_op jit(solution)/shard_map/while/body/eval_jaxpr/cond
  81.9 5.1 %copy-start.5 = (bf16[2048,2,64]{0,2,1:T(8,128)(2,1)S(1)}, bf16[2048,2,64]{0,2,1:T(8,128)(2,1)}, u32[]{:S(2)}) copy-start(bf16[2048,2,64]{0,2,1:T(8,128)(2,1)} %get-tuple-element.872) | copy-start | bytes 1572868 | tf_op jit(solution)/shard_map/while/body/eval_jaxpr/cond
  94.9 4.7 %copy-start.1 = (f32[2,256,512]{1,2,0:T(8,128)S(1)}, f32[2,256,512]{1,2,0:T(8,128)}, u32[]{:S(2)}) copy-start(f32[2,256,512]{1,2,0:T(8,128)} %get-tuple-element.1138) | copy-start | bytes 3145732 | tf_op jit(solution)/shard_map/while/body/eval_jaxpr/cond
  94.9 5.4 %copy-start.18 = (f32[2,256]{1,0:T(2,128)S(1)}, f32[2,256]{1,0:T(2,128)}, u32[]{:S(2)}) copy-start(f32[2,256]{1,0:T(2,128)} %copy-done.17) | copy-start | bytes 6148 | tf_op jit(solution)/shard_map/while/body/eval_jaxpr/cond
  94.9 8.0 %copy-start.3 = (bf16[2048,2,128]{0,2,1:T(8,128)(2,1)S(1)}, bf16[2048,2,128]{0,2,1:T(8,128)(2,1)}, u32[]{:S(2)}) copy-start(bf16[2048,2,128]{0,2,1:T(8,128)(2,1)} %get-tuple-element.863) | copy-start | bytes 3145732 | tf_op jit(solution)/shard_map/while/body/eval_jaxpr/cond
  94.9 8.0 %copy-start.10 = (f32[256,2,128]{0,2,1:T(8,128)S(1)}, f32[256,2,128]{0,2,1:T(8,128)}, u32[]{:S(2)}) copy-start(f32[256,2,128]{0,2,1:T(8,128)} %get-tuple-element.865) | copy-start | bytes 786436 | tf_op jit(solution)/shard_map/while/body/eval_jaxpr/cond
  94.9 8.0 %copy-start.19 = (f32[256,2]{0,1:T(2,128)S(1)}, f32[256,2]{0,1:T(2,128)}, u32[]{:S(2)}) copy-start(f32[256,2]{0,1:T(2,128)} %get-tuple-element.1107) | copy-start | bytes 6148 | tf_op jit(solution)/shard_map/while/body/eval_jaxpr/cond
  98.2 5.1 %copy-start.5 = (bf16[2048,2,64]{0,2,1:T(8,128)(2,1)S(1)}, bf16[2048,2,64]{0,2,1:T(8,128)(2,1)}, u32[]{:S(2)}) copy-start(bf16[2048,2,64]{0,2,1:T(8,128)(2,1)} %get-tuple-element.872) | copy-start | bytes 1572868 | tf_op jit(solution)/shard_map/while/body/eval_jaxpr/cond
  111.2 4.7 %copy-start.1 = (f32[2,256,512]{1,2,0:T(8,128)S(1)}, f32[2,256,512]{1,2,0:T(8,128)}, u32[]{:S(2)}) copy-start(f32[2,256,512]{1,2,0:T(8,128)} %get-tuple-element.1138) | copy-start | bytes 3145732 | tf_op jit(solution)/shard_map/while/body/eval_jaxpr/cond
  111.2 5.4 %copy-start.18 = (f32[2,256]{1,0:T(2,128)S(1)}, f32[2,256]{1,0:T(2,128)}, u32[]{:S(2)}) copy-start(f32[2,256]{1,0:T(2,128)} %copy-done.17) | copy-start | bytes 6148 | tf_op jit(solution)/shard_map/while/body/eval_jaxpr/cond
  111.2 8.0 %copy-start.3 = (bf16[2048,2,128]{0,2,1:T(8,128)(2,1)S(1)}, bf16[2048,2,128]{0,2,1:T(8,128)(2,1)}, u32[]{:S(2)}) copy-start(bf16[2048,2,128]{0,2,1:T(8,128)(2,1)} %get-tuple-element.863) | copy-start | bytes 3145732 | tf_op jit(solution)/shard_map/while/body/eval_jaxpr/cond
  111.2 8.0 %copy-start.10 = (f32[256,2,128]{0,2,1:T(8,128)S(1)}, f32[256,2,128]{0,2,1:T(8,128)}, u32[]{:S(2)}) copy-start(f32[256,2,128]{0,2,1:T(8,128)} %get-tuple-element.865) | copy-start | bytes 786436 | tf_op jit(solution)/shard_map/while/body/eval_jaxpr/cond
  111.2 8.0 %copy-start.19 = (f32[256,2]{0,1:T(2,128)S(1)}, f32[256,2]{0,1:T(2,128)}, u32[]{:S(2)}) copy-start(f32[256,2]{0,1:T(2,128)} %get-tuple-element.1107) | copy-start | bytes 6148 | tf_op jit(solution)/shard_map/while/body/eval_jaxpr/cond
  114.6 5.1 %copy-start.5 = (bf16[2048,2,64]{0,2,1:T(8,128)(2,1)S(1)}, bf16[2048,2,64]{0,2,1:T(8,128)(2,1)}, u32[]{:S(2)}) copy-start(bf16[2048,2,64]{0,2,1:T(8,128)(2,1)} %get-tuple-element.872) | copy-start | bytes 1572868 | tf_op jit(solution)/shard_map/while/body/eval_jaxpr/cond
  127.6 4.7 %copy-start.1 = (f32[2,256,512]{1,2,0:T(8,128)S(1)}, f32[2,256,512]{1,2,0:T(8,128)}, u32[]{:S(2)}) copy-start(f32[2,256,512]{1,2,0:T(8,128)} %get-tuple-element.1138) | copy-start | bytes 3145732 | tf_op jit(solution)/shard_map/while/body/eval_jaxpr/cond
  127.6 5.4 %copy-start.18 = (f32[2,256]{1,0:T(2,128)S(1)}, f32[2,256]{1,0:T(2,128)}, u32[]{:S(2)}) copy-start(f32[2,256]{1,0:T(2,128)} %copy-done.17) | copy-start | bytes 6148 | tf_op jit(solution)/shard_map/while/body/eval_jaxpr/cond
  127.6 8.0 %copy-start.3 = (bf16[2048,2,128]{0,2,1:T(8,128)(2,1)S(1)}, bf16[2048,2,128]{0,2,1:T(8,128)(2,1)}, u32[]{:S(2)}) copy-start(bf16[2048,2,128]{0,2,1:T(8,128)(2,1)} %get-tuple-element.863) | copy-start | bytes 3145732 | tf_op jit(solution)/shard_map/while/body/eval_jaxpr/cond
  127.6 8.0 %copy-start.10 = (f32[256,2,128]{0,2,1:T(8,128)S(1)}, f32[256,2,128]{0,2,1:T(8,128)}, u32[]{:S(2)}) copy-start(f32[256,2,128]{0,2,1:T(8,128)} %get-tuple-element.865) | copy-start | bytes 786436 | tf_op jit(solution)/shard_map/while/body/eval_jaxpr/cond
  127.6 8.0 %copy-start.19 = (f32[256,2]{0,1:T(2,128)S(1)}, f32[256,2]{0,1:T(2,128)}, u32[]{:S(2)}) copy-start(f32[256,2]{0,1:T(2,128)} %get-tuple-element.1107) | copy-start | bytes 6148 | tf_op jit(solution)/shard_map/while/body/eval_jaxpr/cond
  130.9 5.1 %copy-start.5 = (bf16[2048,2,64]{0,2,1:T(8,128)(2,1)S(1)}, bf16[2048,2,64]{0,2,1:T(8,128)(2,1)}, u32[]{:S(2)}) copy-start(bf16[2048,2,64]{0,2,1:T(8,128)(2,1)} %get-tuple-element.872) | copy-start | bytes 1572868 | tf_op jit(solution)/shard_map/while/body/eval_jaxpr/cond
  150.2 4.7 %copy-start.2 = (f32[2,256,512]{1,2,0:T(8,128)S(1)}, f32[2,256,512]{1,2,0:T(8,128)}, u32[]{:S(2)}) copy-start(f32[2,256,512]{1,2,0:T(8,128)} %get-tuple-element.1126) | copy-start | bytes 3145732 | tf_op jit(solution)/shard_map/while/body/eval_jaxpr/cond
  150.2 5.4 %copy-start.16 = (f32[2,256]{1,0:T(2,128)S(1)}, f32[2,256]{1,0:T(2,128)}, u32[]{:S(2)}) copy-start(f32[2,256]{1,0:T(2,128)} %copy-done.15) | copy-start | bytes 6148 | tf_op jit(solution)/shard_map/while/body/eval_jaxpr/cond
  150.2 8.0 %copy-start.4 = (bf16[2048,2,128]{0,2,1:T(8,128)(2,1)S(1)}, bf16[2048,2,128]{0,2,1:T(8,128)(2,1)}, u32[]{:S(2)}) copy-start(bf16[2048,2,128]{0,2,1:T(8,128)(2,1)} %get-tuple-element.809) | copy-start | bytes 3145732 | tf_op jit(solution)/shard_map/while/body/eval_jaxpr/cond
  150.2 8.0 %copy-start.7 = (f32[256,2,128]{0,2,1:T(8,128)S(1)}, f32[256,2,128]{0,2,1:T(8,128)}, u32[]{:S(2)}) copy-start(f32[256,2,128]{0,2,1:T(8,128)} %get-tuple-element.811) | copy-start | bytes 786436 | tf_op jit(solution)/shard_map/while/body/eval_jaxpr/cond
  150.2 8.0 %copy-start.20 = (f32[256,2]{0,1:T(2,128)S(1)}, f32[256,2]{0,1:T(2,128)}, u32[]{:S(2)}) copy-start(f32[256,2]{0,1:T(2,128)} %get-tuple-element.1099) | copy-start | bytes 6148 | tf_op jit(solution)/shard_map/while/body/eval_jaxpr/cond
  153.6 5.1 %copy-start.6 = (bf16[2048,2,64]{0,2,1:T(8,128)(2,1)S(1)}, bf16[2048,2,64]{0,2,1:T(8,128)(2,1)}, u32[]{:S(2)}) copy-start(bf16[2048,2,64]{0,2,1:T(8,128)(2,1)} %get-tuple-element.818) | copy-start | bytes 1572868 | tf_op jit(solution)/shard_map/while/body/eval_jaxpr/cond
  164.7 18.6 %copy-start.14 = (bf16[128,2048]{1,0:T(8,128)(2,1)S(1)}, bf16[128,2048]{1,0:T(8,128)(2,1)}, u32[]{:S(2)}) copy-start(bf16[128,2048]{1,0:T(8,128)(2,1)} %param.39) | copy-start | bytes 1572868
  166.1 18.0 %copy-start.13 = (bf16[256,2048]{1,0:T(8,128)(2,1)S(1)}, bf16[256,2048]{1,0:T(8,128)(2,1)}, u32[]{:S(2)}) copy-start(bf16[256,2048]{1,0:T(8,128)(2,1)} %param.38) | copy-start | bytes 3145732
  169.0 7.5 %collective-permute-start.2 = (bf16[256,384]{0,1:T(8,128)(2,1)S(1)}, bf16[256,384]{0,1:T(8,128)(2,1)S(1)}, u32[]{:S(2)}, u32[]{:S(2)}) collective-permute-start(bf16[256,384]{0,1:T(8,128)(2,1)S(1)} %pad_maximum_fusion.1), channel_id=1, source_target_pairs={{0,8},{8,0},{16,24},{24,16},{1,9},{9,1},{17,25},{25,17},{2,10},{10... | collective-permute-start | bytes 589832 | tf_op jit(solution)/shard_map/ppermute | solution.py:15
  176.5 6.9 %collective-permute-start.3 = (bf16[256,384]{0,1:T(8,128)(2,1)S(1)}, bf16[256,384]{0,1:T(8,128)(2,1)S(1)}, u32[]{:S(2)}, u32[]{:S(2)}) collective-permute-start(bf16[256,384]{0,1:T(8,128)(2,1)S(1)} %collective-permute-done.2), channel_id=1, source_target_pairs={{0,16},{8,24},{16,0},{24,8},{1,17},{9,25},{17,1},{25,9},{2,18},{10... | collective-permute-start | bytes 589832 | tf_op jit(solution)/shard_map/ppermute | solution.py:15
  184.1 39.6 %copy-start.12 = (bf16[64,2048]{1,0:T(8,128)(2,1)S(1)}, bf16[64,2048]{1,0:T(8,128)(2,1)}, u32[]{:S(2)}) copy-start(bf16[64,2048]{1,0:T(8,128)(2,1)} %param.27) | copy-start | bytes 786436
  184.1 40.8 %copy-start.22 = (f32[2048]{0:T(1024)S(1)}, f32[2048]{0:T(1024)}, u32[]{:S(2)}) copy-start(f32[2048]{0:T(1024)} %param.40) | copy-start | bytes 24580
  186.3 116.5 %all-gather.8.cloned.1.call-start = ((), (), s32[]{:S(2)}) async-start(), calls=%async_computation.7 | async-start | bytes 7077888 | tf_op jit(solution)/shard_map/all_gather | solution.py:206
  238.6 153.7 %reduce-scatter.5.cloned.1.call-start = ((), (), s32[]{:S(2)}) async-start(), calls=%async_computation.8 | async-start | bytes 7077888 | tf_op jit(solution)/shard_map/reduce_scatter | solution.py:211
  302.7 8.2 %copy-start.24 = (bf16[1536,2048]{1,0:T(8,128)(2,1)S(1)}, bf16[1536,2048]{1,0:T(8,128)(2,1)}, u32[]{:S(2)}) copy-start(bf16[1536,2048]{1,0:T(8,128)(2,1)} %all-gather.8.cloned.1.call-done) | copy-start | bytes 18874372
  302.7 8.2 %copy-start.25 = (bf16[1,2048,768]{2,1,0:T(8,128)(2,1)S(1)}, bf16[1,2048,768]{2,1,0:T(8,128)(2,1)}, u32[]{:S(2)}) copy-start(bf16[1,2048,768]{2,1,0:T(8,128)(2,1)} %param.44) | copy-start | bytes 9437188
  323.7 73.1 %copy-start.23 = (f32[64,2]{0,1:T(2,128)S(1)}, f32[64,2]{0,1:T(2,128)}, u32[]{:S(2)}) copy-start(f32[64,2]{0,1:T(2,128)} %param.42) | copy-start | bytes 1540
  392.3 13.5 %all-to-all-start.1 = ((bf16[4,48,2048]{2,1,0:T(8,128)(2,1)}), bf16[4,48,2048]{2,1,0:T(8,128)(2,1)}, u32[]{:S(2)}, u32[]{:S(2)}) async-start(bf16[4,48,2048]{2,1,0:T(8,128)(2,1)} %bitcast.128), calls=%async_computation.3 | async-start | bytes 1572864 | tf_op jit(solution)/shard_map/all_to_all | solution.py:220
  (12 other events, 34.3 us)
Sparse Core Ops, SparseCore 0:
  9.2 32.6 all-gather.3
  43.7 26.7 all-gather.5
  186.4 37.3 reduce-scatter.2
  238.7 63.9 all-gather.7
  323.8 68.3 reduce-scatter.4
where the time goes:
time: 425 us; the launch traced here: 423 us
  waiting for transfers between devices  208 us (49%)
  matrix products  78.7 us (19%)
  blocking collectives  39.1 us (9%)
  other arithmetic  36.5 us (9%)
  local copies, waits for them, and re-layouts  27.2 us (6%)
  starting transfers between devices  14.5 us (3%)
  between operations  13.5 us (3%)
  loops' own time  5.82 us (1%)
    reduce_scatter x2, waiting for transfers between devices, per_device(): lax.psum_scatter(lax.optimization_barrier(term.astype(jnp.bfloat16)).asty...  105 us
    all_gather x1, waiting for transfers between devices, per_device(): lax.all_gather(arrived.reshape(sp_ways * capacity, width), 'tp', axis=0,...  63.9 us
    dot_general x20, matrix products, map_update(): jnp.einsum('qhd,khd->hqk', query, keys, preferred_element_type=jnp.float32)  30.7 us
    dot_general x20, matrix products, map_update(): jnp.einsum('hqk,khv->qhv', weights.astype(jnp.bfloat16), values, preferre...  22.8 us
    all_gather x1, waiting for transfers between devices, per_device(): lax.all_gather(value_a, 'sp', axis=0, tiled=True)  17.1 us
    all_gather x1, blocking collectives, per_device(): lax.all_gather(key_b, 'sp', axis=0, tiled=True)  16.1 us
    ppermute x4, waiting for transfers between devices, partner(): lax.ppermute(value, axis, [(i, i ^ 1 << apart) for i in range(lax.axis_si...  13.2 us
    add x10, other arithmetic, map_update(): sums = sums * factor + jnp.sum(weights, axis=2)  12.9 us
  transfers between devices with their start and end apart: 10, of which 8 were waited for; matrix products, arithmetic and copies ran while one was open for 2% of the time, Pallas kernels for 0%

commit v1 on v0

--- a/solution.py
+++ b/solution.py
@@ -3,6 +3,8 @@
 import jax
 import jax.numpy as jnp
 from jax import lax
+from jax.experimental import pallas as pl
+from jax.experimental.pallas import tpu as pltpu
 from jax.sharding import PartitionSpec as P
 
 EPS = 1e-06
@@ -107,6 +109,175 @@
     mixed = outputs[0] - mix[None, :, None] * outputs[1]
     normed = rms_scaled(mixed, gain) * HEAD_SCALE
     return normed.astype(jnp.bfloat16).reshape(mixed.shape[0], -1)
+
+
+def attend_kernel(scalars, packed, rows, out, scores, *, step, width):
+    place = pl.program_id(0)
+    coef = scalars[0]
+    query = packed[pl.ds(place * step, step), 0:width]
+    queries = [query * rows[which : which + 1, :].astype(jnp.bfloat16) for which in range(2)]
+    outputs = []
+
+    def fold(values, combine):
+        parts = [values[:, at * width : (at + 1) * width] for at in range(step // width)]
+        while len(parts) > 1:
+            parts = [combine(*parts[at : at + 2]) for at in range(0, len(parts), 2)]
+        return parts[0]
+
+    def raw(which, index):
+        keys = packed[pl.ds(index * step, step), width : 2 * width]
+        return lax.dot_general(
+            queries[which], keys, (((1,), (1,)), ((), ())), preferred_element_type=jnp.float32
+        )
+
+    row = lax.broadcasted_iota(jnp.int32, (step, step), 0)
+    column = lax.broadcasted_iota(jnp.int32, (step, step), 1)
+    allowed = column <= row
+    highest = []
+    for which in range(2):
+        own = jnp.where(allowed, raw(which, place), NEG)
+        scores[which, place] = own
+        highest.append(fold(own, jnp.maximum))
+
+    def first_pass(index, carry):
+        found = []
+        for which in range(2):
+            block = raw(which, index)
+            scores[which, index] = block
+            found.append(jnp.maximum(carry[which], fold(block, jnp.maximum)))
+        return tuple(found)
+
+    highest = lax.fori_loop(0, place, first_pass, tuple(highest))
+    tops = [jnp.max(found, axis=1, keepdims=True) * coef for found in highest]
+
+    def second_pass(index, carry):
+        values = packed[pl.ds(index * step, step), 2 * width : 3 * width]
+        found = []
+        for which in range(2):
+            total, mixed = carry[which]
+            weights = jnp.exp2(scores[which, index] * coef - tops[which])
+            total = total + fold(weights, jnp.add)
+            mixed = mixed + jnp.dot(
+                weights.astype(jnp.bfloat16), values, preferred_element_type=jnp.float32
+            )
+            found.append((total, mixed))
+        return tuple(found)
+
+    empty = jnp.zeros((step, width), jnp.float32)
+    found = lax.fori_loop(0, place + 1, second_pass, ((empty, empty), (empty, empty)))
+    outputs = [mixed / jnp.sum(total, axis=1, keepdims=True) for total, mixed in found]
+    mixed = outputs[0] - scalars[1] * outputs[1]
+    square = jnp.sum(mixed * mixed, axis=1, keepdims=True) * scalars[2]
+    out[0] = (mixed * lax.rsqrt(square + EPS) * rows[2:3, :]).astype(jnp.bfloat16)
+
+
+def widen(values, width):
+    missing = width - values.shape[-1]
+    return jnp.pad(values, [(0, 0)] * (values.ndim - 1) + [(0, missing)]) if missing else values
+
+
+def exchanged_attention(query_a, key_a, value_a, query_b, key_b, value_b, mix_a, mix_b, head_gain_a, head_gain_b):
+    seq_rows, heads_a, _ = query_a.shape
+    ways = lax.axis_size("sp")
+    place = lax.axis_index("sp")
+    groups = ((query_a, key_a, value_a), (query_b, key_b, value_b))
+    widest = max(array.shape[2] for group in groups for array in group)
+    width = -(-widest // 128) * 128
+    outgoing = jnp.concatenate(
+        [
+            jnp.concatenate([jnp.transpose(widen(array, width), (1, 0, 2)) for array in group], axis=2)
+            for group in groups
+        ],
+        axis=0,
+    )
+    arrived = lax.all_to_all(outgoing, "sp", split_axis=0, concat_axis=0, tiled=True)
+    packed = arrived.reshape(ways * seq_rows, 3 * width)
+    first = place < heads_a
+    maps = jnp.where(first, query_a.shape[2] // 2, query_b.shape[2] // 2)
+    lanes = jnp.arange(width, dtype=jnp.int32)
+    gain = jnp.where(first, widen(head_gain_a, width), widen(head_gain_b, width)) * HEAD_SCALE
+    rows = jnp.stack(
+        [(lanes < maps).astype(jnp.float32), ((lanes >= maps) & (lanes < 2 * maps)).astype(jnp.float32), gain]
+    )
+    coef_a, coef_b = [math.log2(math.e) / math.sqrt(group[0].shape[2] // 2) for group in groups]
+    scalars = jnp.stack(
+        [
+            jnp.where(first, coef_a, coef_b).astype(jnp.float32),
+            lax.dynamic_index_in_dim(jnp.concatenate([mix_a, mix_b]), place, 0, False),
+            jnp.where(first, 1.0 / value_a.shape[2], 1.0 / value_b.shape[2]).astype(jnp.float32),
+        ]
+    )
+    mixed = pl.pallas_call(
+        lambda *refs: attend_kernel(*refs, step=seq_rows, width=width),
+        grid=(ways,),
+        in_specs=[
+            pl.BlockSpec(memory_space=pltpu.SMEM),
+            pl.BlockSpec(packed.shape, lambda index: (0, 0)),
+            pl.BlockSpec(rows.shape, lambda index: (0, 0)),
+        ],
+        out_specs=pl.BlockSpec((1, seq_rows, width), lambda index: (index, 0, 0)),
+        out_shape=jax.ShapeDtypeStruct((ways, seq_rows, width), jnp.bfloat16),
+        scratch_shapes=[pltpu.VMEM((2, ways, seq_rows, seq_rows), jnp.float32)],
+        compiler_params=pltpu.CompilerParams(dimension_semantics=("arbitrary",)),
+        name="attend",
+    )(scalars, packed, rows)
+    return lax.all_to_all(mixed, "sp", split_axis=0, concat_axis=0, tiled=True)
+
+
+def widened_rows(proj, heads, width):
+    per_head = proj.reshape(heads, -1, proj.shape[1])
+    return jnp.pad(per_head, ((0, 0), (0, width - per_head.shape[1]), (0, 0)))
+
+
+def gathered_attention(query_a, key_a, value_a, query_b, key_b, value_b, mix_a, mix_b, head_gain_a, head_gain_b):
+    seq_rows = query_a.shape[0]
+    sp_ways = lax.axis_size("sp")
+    place = lax.axis_index("sp")
+    positions = place * seq_rows + jnp.arange(seq_rows, dtype=jnp.int32)
+    levels = sp_ways.bit_length() - 1
+    half = seq_rows // 2
+    moved = jnp.concatenate(
+        [query_a[half:].reshape(half, -1), query_b[half:].reshape(half, -1)], axis=1
+    )
+    for bit in range(levels):
+        moved = partner(moved, "sp", bit)
+    split_at = query_a.shape[1] * query_a.shape[2]
+    far_a = moved[:, :split_at].reshape(half, query_a.shape[1], query_a.shape[2])
+    far_b = moved[:, split_at:].reshape(half, query_b.shape[1], query_b.shape[2])
+    far_pos = (sp_ways - 1 - place) * seq_rows + half + jnp.arange(half, dtype=jnp.int32)
+    query_sets = ((query_a[:half], query_b[:half], positions[:half]), (far_a, far_b, far_pos))
+
+    def fold_keys(carry, pieces):
+        return tuple(
+            (set_update(states, queries, pieces) for states, queries in zip(carry, query_sets))
+        )
+
+    initial = tuple(
+        (
+            (empty_group(queries[0], value_a), empty_group(queries[1], value_b))
+            for queries in query_sets
+        )
+    )
+    results = fold_keys(
+        initial,
+        (
+            lax.all_gather(key_a, "sp", axis=0, tiled=True),
+            lax.all_gather(value_a, "sp", axis=0, tiled=True),
+            lax.all_gather(key_b, "sp", axis=0, tiled=True),
+            lax.all_gather(value_b, "sp", axis=0, tiled=True),
+        ),
+    )
+    finished = [
+        (finish_group(states[0], mix_a, head_gain_a), finish_group(states[1], mix_b, head_gain_b))
+        for states in results
+    ]
+    returned = jnp.concatenate([finished[1][0], finished[1][1]], axis=1)
+    for bit in range(levels):
+        returned = partner(returned, "sp", bit)
+    width_a = finished[0][0].shape[1]
+    heads_out_a = jnp.concatenate([finished[0][0], returned[:, :width_a]], axis=0)
+    heads_out_b = jnp.concatenate([finished[0][1], returned[:, width_a:]], axis=0)
+    return heads_out_a, heads_out_b
 
 
 def per_device(
@@ -130,60 +301,28 @@
     expert_up,
     expert_down,
 ):
-    seq_rows = query_a.shape[0]
     sp_ways = lax.axis_size("sp")
-    place = lax.axis_index("sp")
-    positions = place * seq_rows + jnp.arange(seq_rows, dtype=jnp.int32)
-    levels = sp_ways.bit_length() - 1
-    half = seq_rows // 2
-    moved = jnp.concatenate(
-        [query_a[half:].reshape(half, -1), query_b[half:].reshape(half, -1)], axis=1
-    )
-    for bit in range(levels):
-        moved = partner(moved, "sp", bit)
-    split_at = query_a.shape[1] * query_a.shape[2]
-    far_a = moved[:, :split_at].reshape(half, query_a.shape[1], query_a.shape[2])
-    far_b = moved[:, split_at:].reshape(half, query_b.shape[1], query_b.shape[2])
-    far_pos = (sp_ways - 1 - place) * seq_rows + half + jnp.arange(half, dtype=jnp.int32)
-    query_sets = ((query_a[:half], query_b[:half], positions[:half]), (far_a, far_b, far_pos))
-
-    def fold_keys(carry, pieces):
-        return tuple(
-            (set_update(states, queries, pieces) for states, queries in zip(carry, query_sets))
-        )
-
-    initial = tuple(
-        (
-            (empty_group(queries[0], value_a), empty_group(queries[1], value_b))
-            for queries in query_sets
-        )
-    )
-    results = fold_keys(
-        initial,
-        (
-            lax.all_gather(key_a, "sp", axis=0, tiled=True),
-            lax.all_gather(value_a, "sp", axis=0, tiled=True),
-            lax.all_gather(key_b, "sp", axis=0, tiled=True),
-            lax.all_gather(value_b, "sp", axis=0, tiled=True),
-        ),
-    )
-    finished = [
-        (finish_group(states[0], mix_a, head_gain_a), finish_group(states[1], mix_b, head_gain_b))
-        for states in results
-    ]
-    returned = jnp.concatenate([finished[1][0], finished[1][1]], axis=1)
-    for bit in range(levels):
-        returned = partner(returned, "sp", bit)
-    width_a = finished[0][0].shape[1]
-    heads_out_a = jnp.concatenate([finished[0][0], returned[:, :width_a]], axis=0)
-    heads_out_b = jnp.concatenate([finished[0][1], returned[:, width_a:]], axis=0)
+    attended = (query_a, key_a, value_a, query_b, key_b, value_b, mix_a, mix_b, head_gain_a, head_gain_b)
+    if query_a.shape[1] + query_b.shape[1] == sp_ways:
+        heads_out = exchanged_attention(*attended)
+        head_width = heads_out.shape[2]
+        left = jnp.transpose(heads_out, (1, 0, 2)).reshape(heads_out.shape[1], -1)
+        right = jnp.concatenate(
+            [
+                widened_rows(proj_a, query_a.shape[1], head_width),
+                widened_rows(proj_b, query_b.shape[1], head_width),
+            ]
+        ).reshape(left.shape[1], -1)
+        term = jnp.dot(left, right, preferred_element_type=jnp.float32)
+    else:
+        heads_out_a, heads_out_b = gathered_attention(*attended)
+        term = jnp.dot(heads_out_a, proj_a, preferred_element_type=jnp.float32)
+        term = term + jnp.dot(heads_out_b, proj_b, preferred_element_type=jnp.float32)
     width = resid.shape[1]
     tok_rows = resid.shape[0]
     top_count = route_ids.shape[1]
     capacity = 3 * top_count * tok_rows // (2 * sp_ways)
     own_slots = slot_numbers(route_ids, sp_ways, capacity)
-    term = jnp.dot(heads_out_a, proj_a, preferred_element_type=jnp.float32)
-    term = term + jnp.dot(heads_out_b, proj_b, preferred_element_type=jnp.float32)
     mixed = resid.astype(jnp.float32) + lax.psum_scatter(
         lax.optimization_barrier(term.astype(jnp.bfloat16))
         .astype(jnp.float32)

time: 425 us -> 312 us (0.73)
  matrix products: 78.7 us -> 26.3 us
  other arithmetic: 36.5 us -> 11.3 us
  Pallas kernels: 0 us -> 16.1 us
  blocking collectives: 39.1 us -> 23.6 us
  waiting for transfers between devices: 208 us -> 194 us
  local copies, waits for them, and re-layouts: 27.2 us -> 17.4 us
  loops' own time: 5.82 us -> 0 us
  starting transfers between devices: 14.5 us -> 9.65 us
    dot_general x42 -> x1, matrix products: 56.4 us -> 4.03 us  [per_device(): term = jnp.dot(left, right, preferred_element_type=jnp.float32)]
    all_gather x2 -> x0, blocking collectives: 26.8 us -> none  [the longest x1 16.1 us: per_device(): lax.all_gather(key_b, 'sp', axis=0, tiled=True)]
    all_to_all x0 -> x1, waiting for transfers between devices: none -> 17.4 us  [exchanged_attention(): lax.all_to_all(outgoing, 'sp', split_axis=0, concat_axis=0, tiled=True)]
    all_gather x2 -> x0, waiting for transfers between devices: 17.1 us -> none  [the longest x1 17.1 us: per_device(): lax.all_gather(value_a, 'sp', axis=0, tiled=True)]
    pallas_call x0 -> x1, Pallas kernels: none -> 16.1 us  [exchanged_attention(): pl.pallas_call(lambda *refs: attend_kernel(*refs, step=seq_rows, width=wi...]
    ppermute x4 -> x0, waiting for transfers between devices: 13.2 us -> none  [partner(): lax.ppermute(value, axis, [(i, i ^ 1 << apart) for i in range(lax.axis_si...]
    add x21 -> x0, other arithmetic: 12.9 us -> none  [the longest x10 12.9 us: map_update(): sums = sums * factor + jnp.sum(weights, axis=2)]
    all_to_all x0 -> x1, blocking collectives: none -> 11.6 us  [exchanged_attention(): return lax.all_to_all(mixed, 'sp', split_axis=0, concat_axis=0, tiled=True)]
  transfers between devices with their start and end apart: 10 -> 5, of which waited for: 8 -> 5; matrix products, arithmetic and copies ran while one was open for 2% -> 1% of each run, Pallas kernels for 0% -> 0%
where the time goes in v1:
time: 312 us
  waiting for transfers between devices  194 us (62%)
  matrix products  26.3 us (8%)
  blocking collectives  23.6 us (8%)
  local copies, waits for them, and re-layouts  17.4 us (6%)
  Pallas kernels  16.1 us (5%)
  between operations  13.3 us (4%)
  other arithmetic  11.3 us (4%)
  starting transfers between devices  9.65 us (3%)
    reduce_scatter x2, waiting for transfers between devices, per_device(): lax.psum_scatter(lax.optimization_barrier(term.astype(jnp.bfloat16)).asty...  104 us
    all_gather x1, waiting for transfers between devices, per_device(): lax.all_gather(arrived.reshape(sp_ways * capacity, width), 'tp', axis=0,...  64.1 us
    all_to_all x1, waiting for transfers between devices, exchanged_attention(): lax.all_to_all(outgoing, 'sp', split_axis=0, concat_axis=0, tiled=True)  17.4 us
    pallas_call x1, Pallas kernels, exchanged_attention(): pl.pallas_call(lambda *refs: attend_kernel(*refs, step=seq_rows, width=wi...  16.1 us
    all_to_all x1, blocking collectives, per_device(): lax.all_to_all(outgoing.reshape(sp_ways, capacity, width), 'sp', split_ax...  12 us
    all_to_all x1, blocking collectives, exchanged_attention(): return lax.all_to_all(mixed, 'sp', split_axis=0, concat_axis=0, tiled=True)  11.6 us
    all_to_all x1, waiting for transfers between devices, per_device(): lax.all_to_all(finished_rows, 'sp', split_axis=0, concat_axis=0, tiled=True)  8.81 us
    dot_general x1, matrix products, per_device(): gate = jnp.dot(piece, expert_gate[0], preferred_element_type=jnp.float32)  8.21 us
  transfers between devices with their start and end apart: 5, of which 5 were waited for; matrix products, arithmetic and copies ran while one was open for 1% of the time, Pallas kernels for 0%

profile of v1, /device:TPU:0, one launch (start us, length us, event | category | flops | bytes accessed | tf_op | source)
XLA Modules:
  0.0 311.7 jit_solution(18119203891793240234)
XLA Ops:
  6.5 2.0 copy.34
  8.5 1.8 copy.35
  10.3 1.8 copy.36
  12.2 0.9 pad_bitcast_fusion.2
  13.1 1.0 pad_bitcast_fusion
  14.1 0.0 copy-start.10
  14.1 2.4 maximum_maximum_fusion
  16.5 5.2 %all-to-all-start = ((bf16[4,512,384]{1,2,0:T(8,128)(2,1)}), bf16[4,512,384]{1,2,0:T(8,128)(2,1)}, u32[]{:S(2)}, u32[]{:S(2)}) async-start(bf16[4,512,384]{1,2,0:T(8,128)(2,1)} %maximum_maximum_fusion), calls=%async_computation | async-start | bytes 3145728 | tf_op jit(solution)/shard_map/all_to_all | solution.py:193
  21.7 0.1 pad_maximum_fusion.1
  21.8 0.6 dynamic_slice.4
  22.5 1.2 pad_maximum_fusion.2.refs_0_
  23.7 0.6 pad_maximum_fusion.refs_2_
  24.3 17.4 %all-to-all-done = bf16[4,512,384]{1,2,0:T(8,128)(2,1)} async-done(((bf16[4,512,384]{1,2,0:T(8,128)(2,1)}), bf16[4,512,384]{1,2,0:T(8,128)(2,1)}, u32[]{:S(2)}, u32[]{:S(2)}) %all-to-all-start) | async-done | bytes 1572896 | tf_op jit(solution)/shard_map/all_to_all | solution.py:193
  41.7 2.6 copy.37
  44.3 16.1 %attend.1 = bf16[4,512,128]{2,1,0:T(8,128)(2,1)} custom-call(f32[3]{0:T(128)} %pad_maximum_fusion.2.refs_0_, bf16[2048,384]{1,0:T(8,128)(2,1)} %bitcast.47, f32[3,128]{1,0:T(4,128)} %pad_maximum_fusion.refs_2_), custom_call_target="tpu_custom_call" | custom-call | tf_op jit(solution)/shard_map/attend/pallas_call | solution.py:210
  60.4 11.6 %all_to_all.20 = bf16[4,512,128]{2,1,0:T(8,128)(2,1)S(1)} all-to-all(bf16[4,512,128]{2,1,0:T(8,128)(2,1)} %attend.1), channel_id=1, replica_groups=mesh['sp'=4,'tp'=8] {'sp'}, dimensions={0} | all-to-all | bytes 1048576 | tf_op jit(solution)/shard_map/all_to_all | solution.py:224
  72.0 4.0 %bitcast_convert_fusion = bf16[512,2048]{1,0:T(8,128)(2,1)} fusion(bf16[2,64,2048]{2,1,0:T(8,128)(2,1)} %bitcast.55, bf16[2,128,2048]{2,1,0:T(8,128)(2,1)} %bitcast.54, bf16[4,512,128]{2,1,0:T(8,128)(2,1)S(1)} %all_to_all.20), kind=kOutput, calls=%fused_computation.4 | convolution fusion | flops 1081081856 | bytes 4194304 | tf_op jit(solution)/shard_map/dot_general | solution.py:316
  76.1 0.0 reduce-scatter.3.cloned.1.call-update
  76.1 0.0 all-gather.2.cloned.1.call-start
  76.1 0.1 copy.39
  76.2 0.1 reshape.115
  76.4 0.1 fusion.14
  76.5 0.2 reduce_window_sum.11
  76.6 0.2 select_reduce_fusion
  76.8 0.1 reduce_sum.32
  77.0 0.1 copy.40
  77.1 35.1 %reduce-scatter.3.cloned.1.call-done = bf16[64,2048]{1,0:T(8,128)(2,1)} async-done(((bf16[512,2048]{1,0:T(8,128)(2,1)}), bf16[64,2048]{1,0:T(8,128)(2,1)}) %reduce-scatter.3.cloned.1.call-update) | async-done | bytes 262160 | tf_op jit(solution)/shard_map/reduce_scatter | solution.py:326
  112.2 1.1 multiply_reduce_fusion.1
  113.3 1.4 convolution_convert_fusion.1
  114.7 12.0 %all_to_all.21 = bf16[4,48,2048]{2,1,0:T(8,128)(2,1)} all-to-all(bf16[4,48,2048]{2,1,0:T(8,128)(2,1)S(1)} %bitcast.49), channel_id=1, replica_groups=mesh['sp'=4,'tp'=8] {'sp'}, dimensions={0} | all-to-all | bytes 1572864 | tf_op jit(solution)/shard_map/all_to_all | solution.py:342
  126.7 0.0 all-gather.2.cloned.1.call-update
  126.7 0.0 reduce-scatter.5.cloned.1.call-start
  126.8 64.1 %all-gather.2.cloned.1.call-done = bf16[1536,2048]{1,0:T(8,128)(2,1)} async-done(((bf16[192,2048]{1,0:T(8,128)(2,1)}), bf16[1536,2048]{1,0:T(8,128)(2,1)}) %all-gather.2.cloned.1.call-update) | async-done | bytes 6291472 | tf_op jit(solution)/shard_map/all_gather | solution.py:345
  190.9 8.2 %fusion.3 = f32[1536,768]{1,0:T(8,128)S(1)} fusion(bf16[1536,2048]{1,0:T(8,128)(2,1)} %all-gather.2.cloned.1.call-done, bf16[1,2048,768]{2,1,0:T(8,128)(2,1)} %param.35), kind=kOutput, calls=%fused_computation.8 | convolution fusion | flops 4831838208 | bytes 14155776 | tf_op jit(solution)/shard_map/dot_general | solution.py:346
  199.1 5.6 %multiply_convert_fusion = bf16[1536,768]{1,0:T(8,128)(2,1)S(1)} fusion(f32[1536,768]{1,0:T(8,128)S(1)} %fusion.3, bf16[1536,2048]{1,0:T(8,128)(2,1)S(1)} %copy-done.7, bf16[1,2048,768]{2,1,0:T(8,128)(2,1)S(1)} %copy-done.8), kind=kOutput, calls=%fused_computation.2 | convolution fusion | flops 4838916096 | bytes 16515072 | tf_op jit(solution)/shard_map/dot_general | solution.py:347
  204.7 7.1 %convolution_convert_fusion = bf16[1536,2048]{1,0:T(8,128)(2,1)} fusion(bf16[1536,768]{1,0:T(8,128)(2,1)S(1)} %multiply_convert_fusion, bf16[1,768,2048]{2,1,0:T(8,128)(2,1)S(1)} %copy-done), kind=kOutput, calls=%fused_computation.1 | convolution fusion | flops 4834983936 | bytes 11796480 | tf_op jit(solution)/shard_map/dot_general | solution.py:349
  211.8 0.0 reduce-scatter.5.cloned.1.call-update
  211.8 68.5 %reduce-scatter.5.cloned.1.call-done = bf16[192,2048]{1,0:T(8,128)(2,1)} async-done(((bf16[1536,2048]{1,0:T(8,128)(2,1)}), bf16[192,2048]{1,0:T(8,128)(2,1)}) %reduce-scatter.5.cloned.1.call-update) | async-done | bytes 786448 | tf_op jit(solution)/shard_map/reduce_scatter | solution.py:350
  280.4 4.4 %all-to-all-start.3 = ((bf16[4,48,2048]{2,1,0:T(8,128)(2,1)}), bf16[4,48,2048]{2,1,0:T(8,128)(2,1)}, u32[]{:S(2)}, u32[]{:S(2)}) async-start(bf16[4,48,2048]{2,1,0:T(8,128)(2,1)} %bitcast.53), calls=%async_computation.5 | async-start | bytes 1572864 | tf_op jit(solution)/shard_map/all_to_all | solution.py:359
  284.8 0.1 copy.42
  284.9 0.1 mul.80
  285.0 0.1 copy.41
  285.1 0.1 copy.38
  285.2 8.8 %all-to-all-done.3 = bf16[4,48,2048]{2,1,0:T(8,128)(2,1)} async-done(((bf16[4,48,2048]{2,1,0:T(8,128)(2,1)}), bf16[4,48,2048]{2,1,0:T(8,128)(2,1)}, u32[]{:S(2)}, u32[]{:S(2)}) %all-to-all-start.3) | async-done | bytes 786464 | tf_op jit(solution)/shard_map/all_to_all | solution.py:359
  294.0 3.5 %gather_fusion = bf16[128,2048]{1,0:T(8,128)(2,1)} fusion(bf16[192,2048]{1,0:T(8,128)(2,1)} %bitcast.22, s32[1024]{0:T(1024)S(1)} %pad_clamp_fusion), kind=kCustom, calls=%fused_computation | custom fusion | bytes 1049088 | tf_op jit(solution)/shard_map/jit(_take)/gather | solution.py:360
  297.5 2.2 gather.7
  299.7 3.7 %multiply_reduce_fusion = f32[64,2048]{1,0:T(8,128)S(1)} fusion(bf16[64,2,2048]{2,1,0:T(2,128)(2,1)} %gather.7, pred[64,2]{1,0:T(8,128)(4,1)S(1)} %copy.41, f32[64,2]{1,0:T(8,128)S(1)} %copy.38), kind=kLoop, calls=%fused_computation.17 | loop fusion | flops 917504 | bytes 1049216 | tf_op jit(solution)/shard_map/reduce_sum | solution.py:362
  303.4 1.8 add_convert_fusion
  (30 shorter events, 0.1 us)
Async XLA Ops:
  6.5 198.2 %copy-start = (bf16[1,768,2048]{2,1,0:T(8,128)(2,1)S(1)}, bf16[1,768,2048]{2,1,0:T(8,128)(2,1)}, u32[]{:S(2)}) copy-start(bf16[1,768,2048]{2,1,0:T(8,128)(2,1)} %param.37) | copy-start | bytes 9437188
  14.1 7.6 %copy-start.9 = (f32[2]{0:T(128)S(1)}, f32[2]{0:T(128)}, u32[]{:S(2)}) copy-start(f32[2]{0:T(128)} %param.27) | copy-start | bytes 28
  14.1 7.6 %copy-start.10 = (f32[2]{0:T(128)S(1)}, f32[2]{0:T(128)}, u32[]{:S(2)}) copy-start(f32[2]{0:T(128)} %param.26) | copy-start | bytes 28
  14.1 9.5 %copy-start.5 = (f32[128]{0:T(128)S(1)}, f32[128]{0:T(128)}, u32[]{:S(2)}) copy-start(f32[128]{0:T(128)} %param.28) | copy-start | bytes 1540
  14.1 9.5 %copy-start.6 = (f32[64]{0:T(128)S(1)}, f32[64]{0:T(128)}, u32[]{:S(2)}) copy-start(f32[64]{0:T(128)} %param.29) | copy-start | bytes 772
  16.5 25.2 %all-to-all-start = ((bf16[4,512,384]{1,2,0:T(8,128)(2,1)}), bf16[4,512,384]{1,2,0:T(8,128)(2,1)}, u32[]{:S(2)}, u32[]{:S(2)}) async-start(bf16[4,512,384]{1,2,0:T(8,128)(2,1)} %maximum_maximum_fusion), calls=%async_computation | async-start | bytes 3145728 | tf_op jit(solution)/shard_map/all_to_all | solution.py:193
  21.7 90.5 %reduce-scatter.3.cloned.1.call-start = ((), (), s32[]{:S(2)}) async-start(), calls=%async_computation.6 | async-start | bytes 2359296 | tf_op jit(solution)/shard_map/reduce_scatter | solution.py:326
  72.0 4.1 %copy-start.2 = (s32[64,2]{0,1:T(2,128)S(1)}, s32[64,2]{0,1:T(2,128)}, u32[]{:S(2)}) copy-start(s32[64,2]{0,1:T(2,128)} %param.33) | copy-start | bytes 1540
  72.0 40.2 %copy-start.1 = (bf16[64,2048]{1,0:T(8,128)(2,1)S(1)}, bf16[64,2048]{1,0:T(8,128)(2,1)}, u32[]{:S(2)}) copy-start(bf16[64,2048]{1,0:T(8,128)(2,1)} %param.19) | copy-start | bytes 786436
  72.0 41.3 %copy-start.3 = (f32[2048]{0:T(1024)S(1)}, f32[2048]{0:T(1024)}, u32[]{:S(2)}) copy-start(f32[2048]{0:T(1024)} %param.32) | copy-start | bytes 24580
  76.1 114.8 %all-gather.2.cloned.1.call-start = ((), (), s32[]{:S(2)}) async-start(), calls=%async_computation.7 | async-start | bytes 7077888 | tf_op jit(solution)/shard_map/all_gather | solution.py:345
  126.7 153.7 %reduce-scatter.5.cloned.1.call-start = ((), (), s32[]{:S(2)}) async-start(), calls=%async_computation.8 | async-start | bytes 7077888 | tf_op jit(solution)/shard_map/reduce_scatter | solution.py:350
  190.9 8.2 %copy-start.7 = (bf16[1536,2048]{1,0:T(8,128)(2,1)S(1)}, bf16[1536,2048]{1,0:T(8,128)(2,1)}, u32[]{:S(2)}) copy-start(bf16[1536,2048]{1,0:T(8,128)(2,1)} %all-gather.2.cloned.1.call-done) | copy-start | bytes 18874372
  190.9 8.2 %copy-start.8 = (bf16[1,2048,768]{2,1,0:T(8,128)(2,1)S(1)}, bf16[1,2048,768]{2,1,0:T(8,128)(2,1)}, u32[]{:S(2)}) copy-start(bf16[1,2048,768]{2,1,0:T(8,128)(2,1)} %param.36) | copy-start | bytes 9437188
  211.8 73.3 %copy-start.4 = (f32[64,2]{0,1:T(2,128)S(1)}, f32[64,2]{0,1:T(2,128)}, u32[]{:S(2)}) copy-start(f32[64,2]{0,1:T(2,128)} %param.34) | copy-start | bytes 1540
  280.4 13.7 %all-to-all-start.3 = ((bf16[4,48,2048]{2,1,0:T(8,128)(2,1)}), bf16[4,48,2048]{2,1,0:T(8,128)(2,1)}, u32[]{:S(2)}, u32[]{:S(2)}) async-start(bf16[4,48,2048]{2,1,0:T(8,128)(2,1)} %bitcast.53), calls=%async_computation.5 | async-start | bytes 1572864 | tf_op jit(solution)/shard_map/all_to_all | solution.py:359
Sparse Core Ops, SparseCore 0:
  76.2 35.9 reduce-scatter.2
  126.8 63.9 all-gather.1
  212.0 68.3 reduce-scatter.4
